TPU v7x, 32 devices: a whole 2x2x4 slice. The times are simulated.
32 devices in a mesh: kv: 8 (over z, y), tp: 4 (over x, core).
Axes of the slice: x: 2, y: 2, z: 4, core: 2. Of those that a mesh axis runs over, the one named last changes fastest.
Arguments:
- tokens: bfloat16 [64, 2048], replicated, may hold values from -60 to 60
- mix_gain: float32 [2048], replicated, may hold values from 0.1 to 1.9
- query_weight: bfloat16 [2048, 1024], P(None, 'tp'), may hold values from -0.125 to 0.125
- key_weight: bfloat16 [2048, 1024], P(None, 'tp'), may hold values from -0.125 to 0.125
- value_weight: bfloat16 [2048, 1024], P(None, 'tp'), may hold values from -0.125 to 0.125
- gate_weight: bfloat16 [2048, 16], replicated, may hold values from -0.125 to 0.125
- gate_bias: float32 [16], replicated, may hold values from -1 to 3
- query_gain: float32 [64], replicated, may hold values from 0.1 to 1.9
- key_gain: float32 [64], replicated, may hold values from 0.1 to 1.9
- cache_keys: bfloat16 [4, 4096, 1024], P(None, 'kv', 'tp'), may hold values from -6 to 6
- cache_values: bfloat16 [4, 4096, 1024], P(None, 'kv', 'tp'), may hold values from -6 to 6
- cached_gates: float32 [4, 16, 4096], P(None, 'tp', 'kv'), as said below
- filled: int32 [4], replicated, may hold values from 1024 to 4063
- accepted: int32 [4], replicated, may hold values from 0 to 16
- parents: int32 [4, 16], replicated, may hold values from -1 to 14, as said below
- out_weight: bfloat16 [1024, 2048], P('tp', 'kv'), may hold values from -0.1875 to 0.1875
Outputs:
- mixed: bfloat16 [64, 2048], P('tp', 'kv')
- new_keys: bfloat16 [4, 4096, 1024], P(None, 'kv', 'tp')
- new_values: bfloat16 [4, 4096, 1024], P(None, 'kv', 'tp')
- new_gates: float32 [4, 16, 4096], P(None, 'tp', 'kv')
Inputs may be any that keep to these rules, and one draw needn't show every extreme that they name: cached_gates[b, h, p] never rises as p grows. parents[b, 0] is -1 and, for t of 1 or more, parents[b, t] lies in 0 to t - 1, so a sequence's proposals form a tree.
All inputs are finite; a program needn't handle non-finite values.
Results may differ from a plain program's by a relative error of at most 0.013.
Values may be sent and summed in bfloat16 or wider, within the bound.
A program may use at most 64 MiB of HBM per device.

v0:
```python
from functools import partial

import jax
import jax.numpy as jnp
from jax import lax
from jax.sharding import PartitionSpec as P

epsilon = 1e-06


def ancestry(parents):
    length = parents.shape[1]
    labels = jnp.arange(length, dtype=jnp.int32)
    start_nodes = jnp.broadcast_to(labels[None, :], parents.shape)
    start_running = (start_nodes[:, :, None] == labels[None, None, :]).astype(jnp.float32)

    def climb_once(step, carry):
        nodes, running = carry
        lifted = jnp.take_along_axis(parents, jnp.maximum(nodes, 0), axis=1)
        nodes = jnp.where(nodes >= 0, lifted, -1)
        running = running + (nodes[:, :, None] == labels[None, None, :]).astype(jnp.float32)
        return (nodes, running)

    finished = lax.fori_loop(0, length - 1, climb_once, (start_nodes, start_running))
    return finished[1]


def climb_sum(ancestors, log_gates):
    return jnp.sum(ancestors[:, :, :, None] * log_gates[:, None, :, :], axis=2)


def head_norm(values, head_gain):
    return (
        values * lax.rsqrt(jnp.mean(values * values, axis=-1, keepdims=True) + epsilon) * head_gain
    ).astype(jnp.bfloat16)


def normalize(numerator, denominator):
    row_total, head_total = denominator.shape
    return (
        (numerator.reshape(row_total, head_total, -1) / denominator[:, :, None])
        .reshape(row_total, -1)
        .astype(jnp.bfloat16)
    )


def write_rows(previous, incoming, offset, along):
    proposals = incoming.shape[along]
    length = previous.shape[along]
    landing = jnp.clip(offset + proposals, 0, length + proposals)
    padded_shape = list(previous.shape)
    padded_shape[along] = length + 2 * proposals
    padded = jnp.zeros(tuple(padded_shape), previous.dtype)
    padded = lax.dynamic_update_slice_in_dim(padded, incoming, landing, along)
    written = jnp.zeros((length + 2 * proposals,), jnp.float32)
    written = lax.dynamic_update_slice_in_dim(
        written, jnp.ones((proposals,), jnp.float32), landing, 0
    )
    mark_shape = [1] * previous.ndim
    mark_shape[along] = length
    written_here = (written[proposals : proposals + length] > 0.5).reshape(tuple(mark_shape))
    kept = lax.slice_in_dim(padded, proposals, proposals + length, axis=along)
    return jnp.where(written_here, kept, previous)


def body(
    tokens,
    mix_gain,
    query_weight,
    key_weight,
    value_weight,
    gate_weight,
    gate_bias,
    query_gain,
    key_gain,
    cache_keys,
    cache_values,
    cached_gates,
    filled,
    accepted,
    parents,
    out_weight,
):
    kv_rank = lax.axis_index("kv")
    head_rank = lax.axis_index("tp")
    row_count, model_width = tokens.shape
    seq_count, pos_count, head_width = cache_keys.shape
    heads_here = cached_gates.shape[1]
    proposals = parents.shape[1]
    head_size = head_width // heads_here
    floats = tokens.astype(jnp.float32)
    row_scale = lax.rsqrt(jnp.mean(floats * floats, axis=1, keepdims=True) + epsilon)
    scaled = (floats * mix_gain).astype(jnp.bfloat16)
    counts = filled + accepted
    positions = kv_rank * pos_count + jnp.arange(pos_count, dtype=jnp.int32)
    at_last = (positions[None, :] == (counts - 1)[:, None]).astype(jnp.float32)
    last_gate = lax.psum(jnp.sum(cached_gates * at_last[:, None, :], axis=2), "kv")
    gate_slice = lax.dynamic_slice_in_dim(gate_weight, head_rank * heads_here, heads_here, 1)
    bias_here = lax.dynamic_slice_in_dim(gate_bias, head_rank * heads_here, heads_here)
    products = (
        jnp.dot(
            scaled,
            jnp.concatenate([query_weight, key_weight, value_weight], axis=1),
            preferred_element_type=jnp.float32,
        )
        * row_scale
    )
    gate_pre = jnp.dot(scaled, gate_slice, preferred_element_type=jnp.float32) * row_scale
    query_heads = head_norm(
        products[:, :head_width].reshape(seq_count, proposals, heads_here, head_size), query_gain
    )
    key_heads = head_norm(
        products[:, head_width : 2 * head_width].reshape(
            seq_count, proposals, heads_here, head_size
        ),
        key_gain,
    )
    value_heads = (
        products[:, 2 * head_width :]
        .astype(jnp.bfloat16)
        .reshape(seq_count, proposals, heads_here, head_size)
    )
    log_gates = jax.nn.log_sigmoid(gate_pre + bias_here).reshape(seq_count, proposals, heads_here)
    ancestors = ancestry(parents)
    climbed = climb_sum(ancestors, log_gates)
    fresh_gates = last_gate[:, None, :] + climbed
    factor = head_size ** (-0.5)
    query_gates = jnp.transpose(fresh_gates, (0, 2, 1))
    joined_keys = jnp.concatenate(
        [cache_keys.reshape(seq_count, pos_count, heads_here, head_size), key_heads], axis=1
    )
    joined_values = jnp.concatenate(
        [cache_values.reshape(seq_count, pos_count, heads_here, head_size), value_heads], axis=1
    )
    joined_gates = jnp.concatenate([cached_gates, query_gates], axis=2)
    is_live = positions[None, :] < counts[:, None]
    on_first = kv_rank == 0
    cache_mask = jnp.broadcast_to(is_live[:, None, :], (seq_count, proposals, pos_count))
    tree_mask = jnp.logical_and(ancestors > 0.5, on_first)
    joined_mask = jnp.concatenate([cache_mask, tree_mask], axis=2)

    def attend_one(inputs):
        query, keys_all, values_all, key_gates, row_gates, mask = inputs
        scores = (
            jnp.einsum("thd,phd->htp", query, keys_all, preferred_element_type=jnp.float32) * factor
        )
        scores = scores + row_gates[:, :, None] - key_gates[:, None, :]
        weights = jnp.where(mask[None], jnp.exp(scores), 0.0)
        denominator_part = jnp.transpose(jnp.sum(weights, axis=2))
        numerator_part = jnp.einsum(
            "htp,phd->thd",
            weights.astype(jnp.bfloat16),
            values_all,
            preferred_element_type=jnp.float32,
        )
        return (numerator_part.reshape(proposals, head_width), denominator_part)

    numerator, denominator = lax.map(
        attend_one,
        (query_heads, joined_keys, joined_values, joined_gates, query_gates, joined_mask),
    )
    numerator_rows = numerator.reshape(row_count, head_width)
    denominator_rows = denominator.reshape(row_count, heads_here)
    numerator_rows, denominator_rows = lax.psum((numerator_rows, denominator_rows), "kv")
    attended = normalize(numerator_rows, denominator_rows)
    mixed = lax.psum_scatter(
        jnp.dot(attended, out_weight, preferred_element_type=jnp.float32).astype(jnp.bfloat16),
        "tp",
        scatter_dimension=0,
        tiled=True,
    )
    offsets = counts - kv_rank * pos_count
    new_keys = jax.vmap(partial(write_rows, along=0))(
        cache_keys, key_heads.reshape(seq_count, proposals, head_width), offsets
    )
    new_values = jax.vmap(partial(write_rows, along=0))(
        cache_values, value_heads.reshape(seq_count, proposals, head_width), offsets
    )
    new_gates = jax.vmap(partial(write_rows, along=1))(cached_gates, query_gates, offsets)
    return (mixed, new_keys, new_values, new_gates)


def solution(mesh):
    return jax.shard_map(
        body,
        mesh=mesh,
        in_specs=(
            P(),
            P(),
            P(None, "tp"),
            P(None, "tp"),
            P(None, "tp"),
            P(),
            P(),
            P(),
            P(),
            P(None, "kv", "tp"),
            P(None, "kv", "tp"),
            P(None, "tp", "kv"),
            P(),
            P(),
            P(),
            P("tp", "kv"),
        ),
        out_specs=(P("tp", "kv"), P(None, "kv", "tp"), P(None, "kv", "tp"), P(None, "tp", "kv")),
        check_vma=False,
    )
```

profile of v0, /device:TPU:0, one launch (start us, length us, event | category | flops | bytes accessed | tf_op | source)
XLA Modules:
  0.0 238.9 jit_solution(14997844388409540507)
XLA Ops:
  8.4 2.7 %fusion.21 = f32[64,768]{1,0:T(8,128)S(1)} fusion(bf16[2048,256]{1,0:T(8,128)(2,1)} %param.24, bf16[2048,256]{1,0:T(8,128)(2,1)} %param.23, bf16[2048,256]{1,0:T(8,128)(2,1)} %param.22, bf16[64,2048]{1,0:T(8,128)(2,1)} %param.20, f32[2048]{0:T(1024)} %param.21, f32[64]{0:T(128)S(1)} %add_rsqrt_fusion.2), kind=kOutput, calls=%fused_computation.45 | convolution fusion | flops 211206144 | bytes 3612928 | tf_op jit(solution)/shard_map/dot_general | solution.py:101
  14.5 17.4 %while.35 = (s32[]{:T(128)}, s32[4,16]{1,0:T(4,128)S(1)}, f32[4,16,16]{2,1,0:T(8,128)S(1)}, s32[4,16]{1,0:T(4,128)S(1)}, s32[]{:T(128)}) while((s32[]{:T(128)}, s32[4,16]{1,0:T(4,128)S(1)}, f32[4,16,16]{2,1,0:T(8,128)S(1)}, s32[4,16]{1,0:T(4,128)S(1)}, s32[]{:T(128)}) %tuple.155), condition=%wide.region_6.7_spmd.clone, body=%wide.region_5.6_spmd.clone.sunk | while | flops 3778 | bytes 11837 | solution.py:24
  35.5 23.2 %psum.21 = f32[4,4]{1,0:T(4,128)S(1)} all-reduce(f32[4,4]{1,0:T(4,128)S(1)} %multiply_reduce_fusion.3), channel_id=1, replica_groups=mesh['kv'=8,'tp'=4] {'kv'}, use_global_device_ids=true, to_apply=%region_4.0 | all-reduce | flops 16 | bytes 128 | tf_op jit(solution)/shard_map/psum | solution.py:97
  60.8 2.5 %pad_maximum_fusion = (bf16[4,528,4,64]{1,3,2,0:T(8,128)(2,1)S(1)}, bf16[4,528,4,64]{1,3,2,0:T(8,128)(2,1)}) fusion(bf16[4,16,4,64]{1,3,2,0:T(8,128)(2,1)} %copy.90, bf16[4,512,4,64]{1,3,2,0:T(8,128)(2,1)S(1)} %bitcast.123, bf16[4,16,4,64]{1,3,2,0:T(8,128)(2,1)} %copy.96, bf16[4,512,4,64]{1,3,2,0:T(8,128)(2,1)S(1)} %bitcast.124), kind=kLoop, calls=%fused_computation.43 | loop fusion | flops 4325376 | bytes 4325376 | tf_op jit(solution)/shard_map/concatenate | solution.py:132
  63.2 19.7 %while.30 = (s32[]{:T(128)}, f32[4,16,256]{2,1,0:T(8,128)}, f32[4,16,4]{1,0,2:T(4,128)}, bf16[4,528,4,64]{1,3,2,0:T(8,128)(2,1)S(1)}, pred[4,16,528]{2,1,0:T(8,1...) while((s32[]{:T(128)}, f32[4,16,256]{2,1,0:T(8,128)}, ...), condition=%wide.region_10.11_spmd, body=%wide.region_8.10_spmd.sunk | while | flops 8853442 | bytes 989325 | solution.py:158
  83.4 28.6 %while.32 = (s32[]{:T(128)}, bf16[4,544,256]{2,1,0:T(8,128)(2,1)S(1)}, s32[4,3]{1,0:T(4,128)S(1)}, bf16[4,16,256]{2,1,0:T(8,128)(2,1)}, s32[]{:T(128)}, /*index=5*/s32[3]{0:T(128)S(1)}, s32[]{:T(128)}) while((s32[]{:T(128)}, bf16[4,544,256]{2,1,0:T(8,128)(2,1)S(1)}, s32[4,3]{1,0:T(4,128)S(1)}, bf16[4,16,256]{2,1,0:T(8,128)(2,1)}, s32[]{:T(128)}, ...), condition=%wide.while_cond.2, body=%wide.while_body.2.sunk | while | flops 4115 | bytes 41139 | solution.py:54
  84.1 2.6 %and_reduce_fusion.9 = pred[]{:T(512)} fusion(s32[3]{0:T(128)S(1)} %get-tuple-element.561, s32[1]{0:T(128)} %bitcast.110, s32[1]{0:T(128)} %bitcast.111, s32[1]{0:T(128)} %bitcast.112), kind=kLoop, calls=%fused_computation.25.clone.1 | loop fusion | flops 17 | bytes 25 | tf_op jit(solution)/shard_map/vmap(vmap())/scatter
  86.7 2.5 %dynamic-slice_select_fusion.7 = bf16[1,16,256]{2,1,0:T(8,128)(2,1)S(1)} fusion(bf16[4,16,256]{2,1,0:T(8,128)(2,1)} %get-tuple-element.559, s32[]{:T(128)S(6)} %copy.151, bf16[4,544,256]{2,1,0:T(8,128)(2,1)S(1)} %get-tuple-element.550, s32[]{:T(128)} %bitcast.108, s32[]{:T(128)} %bitcast.109, pred[]{:T(512)} %and_reduce_fusion.9), kind=kLoop, calls=%fused_computation.24.clone.1 | loop fusion | flops 4096 | bytes 24589 | tf_op jit(solution)/shard_map/vmap(vmap())/scatter
  91.3 2.6 %and_reduce_fusion.9 = pred[]{:T(512)} fusion(s32[3]{0:T(128)S(1)} %get-tuple-element.561, s32[1]{0:T(128)} %bitcast.110, s32[1]{0:T(128)} %bitcast.111, s32[1]{0:T(128)} %bitcast.112), kind=kLoop, calls=%fused_computation.25.clone.1 | loop fusion | flops 17 | bytes 25 | tf_op jit(solution)/shard_map/vmap(vmap())/scatter
  93.9 2.5 %dynamic-slice_select_fusion.7 = bf16[1,16,256]{2,1,0:T(8,128)(2,1)S(1)} fusion(bf16[4,16,256]{2,1,0:T(8,128)(2,1)} %get-tuple-element.559, s32[]{:T(128)S(6)} %copy.151, bf16[4,544,256]{2,1,0:T(8,128)(2,1)S(1)} %get-tuple-element.550, s32[]{:T(128)} %bitcast.108, s32[]{:T(128)} %bitcast.109, pred[]{:T(512)} %and_reduce_fusion.9), kind=kLoop, calls=%fused_computation.24.clone.1 | loop fusion | flops 4096 | bytes 24589 | tf_op jit(solution)/shard_map/vmap(vmap())/scatter
  98.4 2.6 %and_reduce_fusion.9 = pred[]{:T(512)} fusion(s32[3]{0:T(128)S(1)} %get-tuple-element.561, s32[1]{0:T(128)} %bitcast.110, s32[1]{0:T(128)} %bitcast.111, s32[1]{0:T(128)} %bitcast.112), kind=kLoop, calls=%fused_computation.25.clone.1 | loop fusion | flops 17 | bytes 25 | tf_op jit(solution)/shard_map/vmap(vmap())/scatter
  101.0 2.5 %dynamic-slice_select_fusion.7 = bf16[1,16,256]{2,1,0:T(8,128)(2,1)S(1)} fusion(bf16[4,16,256]{2,1,0:T(8,128)(2,1)} %get-tuple-element.559, s32[]{:T(128)S(6)} %copy.151, bf16[4,544,256]{2,1,0:T(8,128)(2,1)S(1)} %get-tuple-element.550, s32[]{:T(128)} %bitcast.108, s32[]{:T(128)} %bitcast.109, pred[]{:T(512)} %and_reduce_fusion.9), kind=kLoop, calls=%fused_computation.24.clone.1 | loop fusion | flops 4096 | bytes 24589 | tf_op jit(solution)/shard_map/vmap(vmap())/scatter
  105.6 2.6 %and_reduce_fusion.9 = pred[]{:T(512)} fusion(s32[3]{0:T(128)S(1)} %get-tuple-element.561, s32[1]{0:T(128)} %bitcast.110, s32[1]{0:T(128)} %bitcast.111, s32[1]{0:T(128)} %bitcast.112), kind=kLoop, calls=%fused_computation.25.clone.1 | loop fusion | flops 17 | bytes 25 | tf_op jit(solution)/shard_map/vmap(vmap())/scatter
  108.2 2.5 %dynamic-slice_select_fusion.7 = bf16[1,16,256]{2,1,0:T(8,128)(2,1)S(1)} fusion(bf16[4,16,256]{2,1,0:T(8,128)(2,1)} %get-tuple-element.559, s32[]{:T(128)S(6)} %copy.151, bf16[4,544,256]{2,1,0:T(8,128)(2,1)S(1)} %get-tuple-element.550, s32[]{:T(128)} %bitcast.108, s32[]{:T(128)} %bitcast.109, pred[]{:T(512)} %and_reduce_fusion.9), kind=kLoop, calls=%fused_computation.24.clone.1 | loop fusion | flops 4096 | bytes 24589 | tf_op jit(solution)/shard_map/vmap(vmap())/scatter
  112.1 24.9 %while.34 = (s32[]{:T(128)}, f32[4,544]{1,0:T(4,128)S(1)}, s32[4,2]{0,1:T(2,128)S(1)}, s32[]{:T(128)}, s32[2]{0:T(128)S(1)}) while((s32[]{:T(128)}, f32[4,544]{1,0:T(4,128)S(1)}, s32[4,2]{0,1:T(2,128)S(1)}, s32[]{:T(128)}, s32[2]{0:T(128)S(1)}) %tuple.161), condition=%wide.while_cond.clone, body=%wide.while_body.sunk.clone.sunk | while | flops 27 | bytes 391 | solution.py:56
  112.7 2.0 and_reduce_fusion.11
  114.7 2.0 broadcast_select_fusion.2
  116.7 1.6 dynamic-update-slice.16
  118.9 2.0 and_reduce_fusion.11
  121.0 2.0 broadcast_select_fusion.2
  123.0 1.6 dynamic-update-slice.16
  125.2 2.0 and_reduce_fusion.11
  127.2 2.0 broadcast_select_fusion.2
  131.4 2.0 and_reduce_fusion.11
  133.4 2.0 broadcast_select_fusion.2
  135.4 1.6 dynamic-update-slice.16
  137.6 26.9 %while.31 = (s32[]{:T(128)}, bf16[4,544,256]{2,1,0:T(8,128)(2,1)S(1)}, s32[4,3]{1,0:T(4,128)S(1)}, bf16[4,16,256]{2,1,0:T(8,128)(2,1)S(1)}, s32[]{:T(128)}, /*index=5*/s32[3]{0:T(128)S(1)}, s32[]{:T(128)}) while((s32[]{:T(128)}, bf16[4,544,256]{2,1,0:T(8,128)(2,1)S(1)}, s32[4,3]{1,0:T(4,128)S(1)}, bf16[4,16,256]{2,1,0:T(8,128)(2,1)S(1)}, s32[]{:T(128)}, ...), condition=%wide.while_cond.1, body=%wide.while_body.1.sunk | while | flops 4115 | bytes 41139 | solution.py:54
  138.2 2.7 %and_reduce_fusion.8 = pred[]{:T(512)} fusion(s32[3]{0:T(128)S(1)} %get-tuple-element.597, s32[1]{0:T(128)} %bitcast.105, s32[1]{0:T(128)} %bitcast.106, s32[1]{0:T(128)} %bitcast.107), kind=kLoop, calls=%fused_computation.22.clone.1 | loop fusion | flops 17 | bytes 25 | tf_op jit(solution)/shard_map/vmap(vmap())/scatter
  140.9 1.9 dynamic-slice_select_fusion.6
  144.9 2.7 %and_reduce_fusion.8 = pred[]{:T(512)} fusion(s32[3]{0:T(128)S(1)} %get-tuple-element.597, s32[1]{0:T(128)} %bitcast.105, s32[1]{0:T(128)} %bitcast.106, s32[1]{0:T(128)} %bitcast.107), kind=kLoop, calls=%fused_computation.22.clone.1 | loop fusion | flops 17 | bytes 25 | tf_op jit(solution)/shard_map/vmap(vmap())/scatter
  147.6 1.9 dynamic-slice_select_fusion.6
  151.6 2.7 %and_reduce_fusion.8 = pred[]{:T(512)} fusion(s32[3]{0:T(128)S(1)} %get-tuple-element.597, s32[1]{0:T(128)} %bitcast.105, s32[1]{0:T(128)} %bitcast.106, s32[1]{0:T(128)} %bitcast.107), kind=kLoop, calls=%fused_computation.22.clone.1 | loop fusion | flops 17 | bytes 25 | tf_op jit(solution)/shard_map/vmap(vmap())/scatter
  154.3 1.9 dynamic-slice_select_fusion.6
  158.3 2.7 %and_reduce_fusion.8 = pred[]{:T(512)} fusion(s32[3]{0:T(128)S(1)} %get-tuple-element.597, s32[1]{0:T(128)} %bitcast.105, s32[1]{0:T(128)} %bitcast.106, s32[1]{0:T(128)} %bitcast.107), kind=kLoop, calls=%fused_computation.22.clone.1 | loop fusion | flops 17 | bytes 25 | tf_op jit(solution)/shard_map/vmap(vmap())/scatter
  161.0 1.9 dynamic-slice_select_fusion.6
  164.5 27.3 %while.33 = (s32[]{:T(128)}, f32[4,4,544]{2,1,0:T(4,128)S(1)}, s32[4,3]{1,0:T(4,128)S(1)}, f32[4,4,16]{2,1,0:T(4,128)S(1)}, s32[]{:T(128)}, /*index=5*/s32[3]{0:T(128)S(1)}, s32[]{:T(128)}) while((s32[]{:T(128)}, f32[4,4,544]{2,1,0:T(4,128)S(1)}, s32[4,3]{1,0:T(4,128)S(1)}, f32[4,4,16]{2,1,0:T(4,128)S(1)}, s32[]{:T(128)}, ...), condition=%wide.while_cond.3, body=%wide.while_body.3.sunk | while | flops 83 | bytes 1459 | solution.py:54
  165.2 2.7 %and_reduce_fusion.10 = pred[]{:T(512)} fusion(s32[3]{0:T(128)S(1)} %get-tuple-element.618, s32[1]{0:T(128)} %bitcast.115, s32[1]{0:T(128)} %bitcast.116, s32[1]{0:T(128)} %bitcast.117), kind=kLoop, calls=%fused_computation.28.clone.1 | loop fusion | flops 17 | bytes 25 | tf_op jit(solution)/shard_map/vmap(vmap())/scatter
  167.8 2.0 dynamic-slice_select_fusion.8
  172.0 2.7 %and_reduce_fusion.10 = pred[]{:T(512)} fusion(s32[3]{0:T(128)S(1)} %get-tuple-element.618, s32[1]{0:T(128)} %bitcast.115, s32[1]{0:T(128)} %bitcast.116, s32[1]{0:T(128)} %bitcast.117), kind=kLoop, calls=%fused_computation.28.clone.1 | loop fusion | flops 17 | bytes 25 | tf_op jit(solution)/shard_map/vmap(vmap())/scatter
  174.6 2.0 dynamic-slice_select_fusion.8
  178.8 2.7 %and_reduce_fusion.10 = pred[]{:T(512)} fusion(s32[3]{0:T(128)S(1)} %get-tuple-element.618, s32[1]{0:T(128)} %bitcast.115, s32[1]{0:T(128)} %bitcast.116, s32[1]{0:T(128)} %bitcast.117), kind=kLoop, calls=%fused_computation.28.clone.1 | loop fusion | flops 17 | bytes 25 | tf_op jit(solution)/shard_map/vmap(vmap())/scatter
  181.5 2.0 dynamic-slice_select_fusion.8
  185.6 2.7 %and_reduce_fusion.10 = pred[]{:T(512)} fusion(s32[3]{0:T(128)S(1)} %get-tuple-element.618, s32[1]{0:T(128)} %bitcast.115, s32[1]{0:T(128)} %bitcast.116, s32[1]{0:T(128)} %bitcast.117), kind=kLoop, calls=%fused_computation.28.clone.1 | loop fusion | flops 17 | bytes 25 | tf_op jit(solution)/shard_map/vmap(vmap())/scatter
  188.3 2.0 dynamic-slice_select_fusion.8
  191.9 2.6 %slice_select_fusion = (bf16[4,512,256]{2,1,0:T(8,128)(2,1)}, bf16[4,512,256]{2,1,0:T(8,128)(2,1)}) fusion(bf16[4,512,256]{2,1,0:T(8,128)(2,1)S(1)} %copy-done.3, bf16[4,544,256]{2,1,0:T(8,128)(2,1)S(1)} %get-tuple-element.103, pred[4,512]{1,0:T(4,128)(4,1)S(1)} %slice_compare_fusion, bf16[4,512,256]{2,1,0:T(8,128)(2,1)} %param.29, ...), kind=kLoop, calls=%fused_computation.50 | loop fusion | flops 1048576 | bytes 6293504 | tf_op jit(solution)/shard_map/vmap(jit(_where))/select_n | solution.py:63
  194.5 17.1 %psum.23 = f32[64,4]{0,1:T(4,128)S(1)} all-reduce(f32[64,4]{0,1:T(4,128)S(1)} %reshape.150), channel_id=1, replica_groups=mesh['kv'=8,'tp'=4] {'kv'}, use_global_device_ids=true, to_apply=%region_12.13 | all-reduce | flops 256 | bytes 2048 | tf_op jit(solution)/shard_map/psum | solution.py:164
  212.1 1.6 convolution_convert_fusion
  214.4 17.7 %reduce-scatter.2.cloned.1.call-done = bf16[16,256]{1,0:T(8,128)(2,1)} async-done(((bf16[64,256]{1,0:T(8,128)(2,1)}), bf16[16,256]{1,0:T(8,128)(2,1)}) %reduce-scatter.2.cloned.1.call-update) | async-done | bytes 8208 | tf_op jit(solution)/shard_map/reduce_scatter | solution.py:166
  (290 shorter events, 78.1 us)
Async XLA Ops:
  7.2 204.9 %copy-start = (bf16[256,256]{1,0:T(8,128)(2,1)S(1)}, bf16[256,256]{1,0:T(8,128)(2,1)}, u32[]{:S(2)}) copy-start(bf16[256,256]{1,0:T(8,128)(2,1)} %param.35) | copy-start | bytes 393220
  7.2 204.9 %all-reduce.4.cloned.1.call-start = ((), (), s32[]{:S(2)}) async-start(), calls=%async_computation.1 | async-start | bytes 131072 | tf_op jit(solution)/shard_map/psum | solution.py:164
  8.4 4.2 %copy-start.2 = (bf16[4,512,256]{2,1,0:T(8,128)(2,1)S(1)}, bf16[4,512,256]{2,1,0:T(8,128)(2,1)}, u32[]{:S(2)}) copy-start(bf16[4,512,256]{2,1,0:T(8,128)(2,1)} %param.30) | copy-start | bytes 3145732
  11.1 0.6 copy-start.7
  11.1 2.1 copy-start.5
  12.6 0.9 copy-start.16
  12.6 1.9 copy-start.1
  14.5 17.5 %copy-start.22 = (s32[4]{0:T(128)S(1)}, s32[4]{0:T(128)}, u32[]{:S(2)}) copy-start(s32[4]{0:T(128)} %param.32) | copy-start | bytes 52
  14.5 17.5 %copy-start.23 = (s32[4]{0:T(128)S(1)}, s32[4]{0:T(128)}, u32[]{:S(2)}) copy-start(s32[4]{0:T(128)} %param.33) | copy-start | bytes 52
  14.5 19.0 %copy-start.25 = (f32[16]{0:T(128)S(1)}, f32[16]{0:T(128)}, u32[]{:S(2)}) copy-start(f32[16]{0:T(128)} %param.26) | copy-start | bytes 196
  14.5 19.1 %copy-start.10 = (bf16[64,2048]{1,0:T(8,128)(2,1)S(1)}, bf16[64,2048]{1,0:T(8,128)(2,1)}, u32[]{:S(2)}) copy-start(bf16[64,2048]{1,0:T(8,128)(2,1)} %param.20) | copy-start | bytes 786436
  14.5 19.1 %copy-start.24 = (f32[2048]{0:T(1024)S(1)}, f32[2048]{0:T(1024)}, u32[]{:S(2)}) copy-start(f32[2048]{0:T(1024)} %param.21) | copy-start | bytes 24580
  14.5 20.4 %copy-start.8 = (f32[4,4,512]{2,1,0:T(4,128)S(1)}, f32[4,4,512]{2,1,0:T(4,128)}, u32[]{:S(2)}) copy-start(f32[4,4,512]{2,1,0:T(4,128)} %param.31) | copy-start | bytes 98308
  14.5 20.5 %copy-start.4 = (bf16[4,512,256]{2,1,0:T(8,128)(2,1)S(1)}, bf16[4,512,256]{2,1,0:T(8,128)(2,1)}, u32[]{:S(2)}) copy-start(bf16[4,512,256]{2,1,0:T(8,128)(2,1)} %param.29) | copy-start | bytes 3145732
  34.6 25.5 %copy-start.12 = (f32[4,16,4]{1,2,0:T(4,128)S(1)}, f32[4,16,4]{1,2,0:T(4,128)}, u32[]{:S(2)}) copy-start(f32[4,16,4]{1,2,0:T(4,128)} %add_rsqrt_fusion.1) | copy-start | bytes 3076
  34.6 25.5 %copy-start.20 = (f32[64]{0:T(128)S(1)}, f32[64]{0:T(128)}, u32[]{:S(2)}) copy-start(f32[64]{0:T(128)} %param.27) | copy-start | bytes 772
  63.2 19.9 %copy-start.18 = (s32[4]{0:T(128)S(1)}, s32[4]{0:T(128)}, u32[]{:S(2)}) copy-start(s32[4]{0:T(128)} %get-tuple-element.265) | copy-start | bytes 52
  63.2 19.9 %copy-start.21 = (s32[2]{0:T(128)S(1)}, s32[2]{0:T(128)}, u32[]{:S(2)}) copy-start(s32[2]{0:T(128)} %constant.106.clone.1) | copy-start | bytes 28
  63.2 20.2 %copy-start.11 = (s32[3]{0:T(128)S(1)}, s32[3]{0:T(128)}, u32[]{:S(2)}) copy-start(s32[3]{0:T(128)} %constant.291) | copy-start | bytes 40
  82.9 29.1 %copy-start.19 = (s32[4,1]{0,1:T(1,128)S(1)}, s32[4,1]{0,1:T(1,128)}, u32[]{:S(2)}) copy-start(s32[4,1]{0,1:T(1,128)} %get-tuple-element.264) | copy-start | bytes 52
  82.9 29.2 %copy-start.14 = (s32[2]{0:T(128)S(1)}, s32[2]{0:T(128)}, u32[]{:S(2)}) copy-start(s32[2]{0:T(128)} %constant.327) | copy-start | bytes 28
  83.0 54.4 %copy-start.17 = (f32[64]{0:T(128)S(1)}, f32[64]{0:T(128)}, u32[]{:S(2)}) copy-start(f32[64]{0:T(128)} %param.28) | copy-start | bytes 772
  83.0 54.5 %copy-start.6 = (f32[64,256]{1,0:T(8,128)S(1)}, f32[64,256]{1,0:T(8,128)}, u32[]{:S(2)}) copy-start(f32[64,256]{1,0:T(8,128)} %copy-done.5) | copy-start | bytes 196612
  83.0 149.1 %reduce-scatter.2.cloned.1.call-start = ((), (), s32[]{:S(2)}) async-start(), calls=%async_computation.2 | async-start | bytes 40960 | tf_op jit(solution)/shard_map/reduce_scatter | solution.py:166
  112.0 52.5 %copy-start.13 = (s32[3]{0:T(128)S(1)}, s32[3]{0:T(128)}, u32[]{:S(2)}) copy-start(s32[3]{0:T(128)} %constant.315) | copy-start | bytes 40
  137.0 54.8 %copy-start.3 = (bf16[4,512,256]{2,1,0:T(8,128)(2,1)S(1)}, bf16[4,512,256]{2,1,0:T(8,128)(2,1)}, u32[]{:S(2)}) copy-start(bf16[4,512,256]{2,1,0:T(8,128)(2,1)} %param.30) | copy-start | bytes 3145732
  191.8 2.6 %copy-start.15 = (f32[4,16,4]{1,0,2:T(4,128)S(1)}, f32[4,16,4]{1,0,2:T(4,128)}, u32[]{:S(2)}) copy-start(f32[4,16,4]{1,0,2:T(4,128)} %get-tuple-element.81) | copy-start | bytes 3076
  191.9 21.8 %copy-start.9 = (f32[4,4,512]{2,1,0:T(4,128)S(1)}, f32[4,4,512]{2,1,0:T(4,128)}, u32[]{:S(2)}) copy-start(f32[4,4,512]{2,1,0:T(4,128)} %param.31) | copy-start | bytes 98308
Sparse Core Ops, SparseCore 0:
  83.1 66.6 all-reduce.3
  213.8 18.2 reduce-scatter.1
where the time goes:
time: 241 us; the launch traced here: 239 us
  other arithmetic  86.1 us (36%)
  local copies, waits for them, and re-layouts  68.4 us (28%)
  blocking collectives  40.3 us (17%)
  waiting for transfers between devices  17.7 us (7%)
  between operations  14.5 us (6%)
  matrix products  11.1 us (5%)
    scatter x32, other arithmetic  73.7 us
    scatter x48, local copies, waits for them, and re-layouts  33.6 us
    psum x1, blocking collectives, body(): lax.psum(jnp.sum(cached_gates * at_last[:, None, :], axis=2), 'kv')  23.2 us
    reduce_scatter x1, waiting for transfers between devices, body(): lax.psum_scatter(jnp.dot(attended, out_weight, preferred_element_type=jnp...  17.7 us
    psum x1, blocking collectives, body(): lax.psum((numerator_rows, denominator_rows), 'kv')  17.1 us
    gather x45, local copies, waits for them, and re-layouts, climb_once(): lifted = jnp.take_along_axis(parents, jnp.maximum(nodes, 0), axis=1)  15.7 us
    dynamic_update_slice x8, local copies, waits for them, and re-layouts, body(): lax.map(attend_one, (query_heads, joined_keys, joined_values, joined_gate...  7.68 us
    dot_general x4, matrix products, attend_one(): jnp.einsum('thd,phd->htp', query, keys_all, preferred_element_type=jnp.fl...  4.99 us
  transfers between devices with their start and end apart: 2, of which 1 were waited for; matrix products, arithmetic and copies ran while one was open for 47% of the time, Pallas kernels for 0%

commit v1 on v0

v1 whole, which is shorter than its diff:
```python
from functools import partial

import jax
import jax.numpy as jnp
from jax import lax
from jax.experimental import pallas as pl
from jax.experimental.pallas import tpu as pltpu
from jax.sharding import PartitionSpec as P

epsilon = 1e-06
SHIFT = 16.0
FAR = float(2.0**100)
LANES = 128
F32 = jnp.float32
BF16 = jnp.bfloat16
HIGH = lax.Precision.HIGHEST
VMEM = pltpu.VMEM


def iota(shape, axis):
    return lax.broadcasted_iota(jnp.int32, shape, axis)


def head_kernel(
    tokens, mix_gain, gate_weight, gate_bias, query_gain, key_gain, gates, parents,
    filled, accepted, wq, wk, wv, cache_keys, cache_values,
    message, tree, base, mask, new_keys, new_values,
    wbuf, kbuf, vbuf, wsem, ksem, vsem, osem,
):
    kv_rank = lax.axis_index("kv")
    tp_rank = lax.axis_index("tp")
    seqs, length, width = kbuf.shape
    heads = gates.shape[1]
    size = width // heads
    props = parents.shape[1]
    rows = seqs * props
    loads = []
    for i, w in enumerate((wq, wk)):
        loads.append(pltpu.make_async_copy(w, wbuf.at[i], wsem.at[i]))
    key_in = [pltpu.make_async_copy(cache_keys.at[b], kbuf.at[b], ksem.at[b]) for b in range(seqs)]
    value_in = [
        pltpu.make_async_copy(cache_values.at[b], vbuf.at[b], vsem.at[b]) for b in range(seqs)
    ]
    loads.append(pltpu.make_async_copy(wv, wbuf.at[2], wsem.at[2]))
    for c in loads[:2] + key_in + loads[2:] + value_in:
        c.start()

    floats = tokens[...].astype(F32)
    row_scale = lax.rsqrt(jnp.mean(floats * floats, axis=1, keepdims=True) + epsilon)
    scaled = (floats * mix_gain[...]).astype(BF16)

    parent_row = jnp.concatenate([parents[b : b + 1, :] for b in range(seqs)], axis=1)
    up = iota((rows, rows), 0)
    across = iota((rows, rows), 1)
    same = (up // props) == (across // props)
    power = (
        jnp.logical_and(same, jnp.broadcast_to(parent_row, (rows, rows)) == up % props)
        .astype(F32)
        .astype(BF16)
    )
    anc = (up == across).astype(F32) + power.astype(F32)
    reach = 2
    while reach < props:
        power = jnp.dot(power, power, preferred_element_type=F32).astype(BF16)
        anc = anc + jnp.dot(anc.astype(BF16), power, preferred_element_type=F32)
        reach *= 2
    ancestors = jnp.transpose(anc)

    gate_pre = jnp.dot(scaled, gate_weight[...], preferred_element_type=F32) * row_scale
    gate_pre = gate_pre + gate_bias[...]
    log_gates = jnp.minimum(gate_pre, 0.0) - jnp.log1p(jnp.exp(-jnp.abs(gate_pre)))
    all_heads = log_gates.shape[1]
    pick = iota((all_heads, LANES), 0) == tp_rank * heads + iota((all_heads, LANES), 1)
    pick = jnp.logical_and(pick, iota((all_heads, LANES), 1) < heads).astype(F32)
    local_gates = jnp.dot(log_gates, pick, preferred_element_type=F32, precision=HIGH)
    climb = jnp.dot(ancestors, local_gates, preferred_element_type=F32, precision=HIGH)
    climb_across = jnp.transpose(climb)

    def normed(full, gain):
        parts = []
        for h in range(heads):
            part = full[:, h * size : (h + 1) * size]
            scale = lax.rsqrt(jnp.mean(part * part, axis=1, keepdims=True) + epsilon)
            parts.append(part * scale * gain)
        return parts

    def project(i):
        loads[i].wait()
        return jnp.dot(scaled, wbuf[i], preferred_element_type=F32) * row_scale

    factor = size ** (-0.5)
    query = [
        (q.astype(BF16).astype(F32) * factor).astype(BF16)
        for q in normed(project(0), query_gain[...])
    ]
    fresh_key_heads = [k.astype(BF16) for k in normed(project(1), key_gain[...])]
    query_all = jnp.concatenate(query, axis=1)
    fresh_keys = jnp.concatenate(fresh_key_heads, axis=1)
    fresh_values = project(2).astype(BF16)

    window = 2 * props
    lane_head = iota((props, width), 1) // size
    block_head = iota((heads * props, width), 1) // size
    block_row = iota((heads * props, width), 0) // props
    diagonal = block_head == block_row
    positions = kv_rank * length + iota((heads, length), 1)
    lane = iota((props, LANES), 1)
    out_copies = []
    refs = []
    for b in range(seqs):
        count = filled[b] + accepted[b]
        live = positions < count
        own = gates[b]
        refs.append(jnp.min(jnp.where(live, own, FAR), axis=1, keepdims=True))
    for b in range(seqs):
        lo = b * props
        count = filled[b] + accepted[b]
        live = positions < count
        own = gates[b]
        ref = refs[b]
        shifted = jnp.where(live, ref - own - SHIFT, -FAR)
        spread = jnp.concatenate(
            [jnp.broadcast_to(shifted[h : h + 1, :], (props, length)) for h in range(heads)], axis=0
        )
        climb_col = jnp.concatenate([climb[lo : lo + props, h : h + 1] for h in range(heads)], axis=0)
        tiled = jnp.concatenate([query_all[lo : lo + props, :]] * heads, axis=0)
        tiled = jnp.where(diagonal, tiled, jnp.zeros_like(tiled))
        key_in[b].wait()
        scores = lax.dot_general(
            tiled, kbuf[b], (((1,), (1,)), ((), ())), preferred_element_type=F32
        )
        weights = jnp.exp(scores + climb_col + spread)
        den = jnp.sum(weights, axis=1, keepdims=True)
        value_in[b].wait()
        full = jnp.dot(weights.astype(BF16), vbuf[b], preferred_element_type=F32)
        num = jnp.zeros((props, width), F32)
        side = jnp.zeros((props, LANES), F32)
        for h in range(heads):
            num = jnp.where(lane_head == h, full[h * props : (h + 1) * props, :], num)
            side = jnp.where(lane == h, den[h * props : (h + 1) * props, :], side)
            side = jnp.where(lane == heads + h, ref[h : h + 1, :], side)
            for other in range(seqs):
                side = jnp.where(
                    lane == (2 + other) * heads + h, refs[other][h : h + 1, :], side
                )
        message[lo : lo + props, :width] = num
        message[lo : lo + props, width:] = side

        offset = count - kv_rank * length
        start = jnp.clip((offset // props) * props, 0, length - window)
        start = pl.multiple_of(start, props)
        rel = start + iota((window, props), 0) - offset
        one_hot = (rel == iota((window, props), 1)).astype(F32).astype(BF16)
        row_rel = start + iota((window, width), 0) - offset
        inside = jnp.logical_and(row_rel >= 0, row_rel < props)
        for fresh, buf, out, i in (
            (fresh_keys, kbuf, new_keys, 0),
            (fresh_values, vbuf, new_values, 1),
        ):
            placed = jnp.dot(one_hot, fresh[lo : lo + props, :], preferred_element_type=F32)
            old = buf[b, pl.ds(start, window), :].astype(F32)
            buf[b, pl.ds(start, window), :] = jnp.where(inside, placed, old).astype(BF16)
            c = pltpu.make_async_copy(buf.at[b], out.at[b], osem.at[i, b])
            c.start()
            out_copies.append(c)

        gate_rel = positions - count
        chosen = jnp.logical_and(gate_rel >= 0, gate_rel < props)
        placed_gates = own
        for t in range(props):
            column = jnp.concatenate(
                [climb[lo + t : lo + t + 1, h : h + 1] for h in range(heads)], axis=0
            )
            placed_gates = jnp.where(gate_rel == t, column, placed_gates)
        base[b] = placed_gates
        mask[b] = chosen.astype(F32)

    tree_side = jnp.zeros((rows, LANES), F32)
    row_lane = iota((rows, LANES), 1)
    tree_parts = []
    for h in range(heads):
        scores = lax.dot_general(
            query[h], fresh_key_heads[h], (((1,), (1,)), ((), ())), preferred_element_type=F32
        )
        scores = scores + climb[:, h : h + 1] - climb_across[h : h + 1, :] - SHIFT
        weights = jnp.exp(jnp.where(ancestors > 0.5, scores, -FAR))
        tree_side = jnp.where(row_lane == h, jnp.sum(weights, axis=1, keepdims=True), tree_side)
        tree_parts.append(
            jnp.dot(
                weights.astype(BF16),
                fresh_values[:, h * size : (h + 1) * size],
                preferred_element_type=F32,
            )
        )
    tree[:, :width] = jnp.concatenate(tree_parts, axis=1)
    tree[:, width:] = tree_side
    for c in out_copies:
        c.wait()


def tail_kernel(
    kv_size, tp_size, heads, message, tree, base, mask, weight,
    mixed, new_gates,
    inbox, attended, rows_in, weights_in, send1, recv1, send2, recv2, send3, recv3,
):
    k = lax.axis_index("kv")
    j = lax.axis_index("tp")
    total = kv_size * tp_size
    me = k * tp_size + j
    piece = message.shape[1]
    width = attended.shape[1]
    size = width // heads
    seqs = base.shape[0]
    slots = rows_in.shape[0]
    per_owner = slots // tp_size
    owner = k // per_owner
    barrier = pltpu.get_barrier_semaphore()

    def greet(s, carry):
        other = lax.rem(me + s, total)
        pl.semaphore_signal(
            barrier, inc=1, device_id={"kv": other // tp_size, "tp": lax.rem(other, tp_size)}
        )
        return carry

    lax.fori_loop(1, total, greet, 0)
    pl.semaphore_wait(barrier, total - 1)

    first = []
    for s in range(1, kv_size):
        dst = lax.rem(k + s, kv_size)
        c = pltpu.make_async_remote_copy(
            src_ref=message.at[dst], dst_ref=inbox.at[k], send_sem=send1.at[s],
            recv_sem=recv1.at[k], device_id={"kv": dst},
        )
        c.start()
        first.append(c)
    third = []
    for s in range(1, tp_size):
        dst = lax.rem(j + s, tp_size)
        c = pltpu.make_async_remote_copy(
            src_ref=weight, dst_ref=weights_in.at[j], send_sem=send3.at[s],
            recv_sem=recv3.at[j], device_id={"tp": dst},
        )
        c.start()
        third.append(c)
    inbox[k] = message[k]
    weights_in[j] = weight[...]
    for s in range(1, kv_size):
        src = lax.rem(k + kv_size - s, kv_size)
        pltpu.make_async_remote_copy(
            src_ref=message.at[src], dst_ref=inbox.at[src], send_sem=send1.at[s],
            recv_sem=recv1.at[src], device_id={"kv": src},
        ).wait_recv()

    last = inbox[0][:, width + heads : width + 2 * heads]
    for i in range(1, kv_size):
        last = jnp.minimum(last, inbox[i][:, width + heads : width + 2 * heads])
    scales = []
    own_tree = tree[k]
    den = own_tree[:, width : width + heads]
    for i in range(kv_size):
        scale = jnp.exp(last - inbox[i][:, width + heads : width + 2 * heads])
        den = den + scale * inbox[i][:, width : width + heads]
        scales.append(scale)

    def spread(x):
        return jnp.concatenate(
            [jnp.broadcast_to(x[:, h : h + 1], (piece, size)) for h in range(heads)], axis=1
        )

    num = own_tree[:, :width]
    for i in range(kv_size):
        num = num + spread(scales[i]) * inbox[i][:, :width]
    result = (num / spread(den)).astype(BF16).astype(F32)
    attended[...] = result

    slot = j * per_owner + lax.rem(k, per_owner)
    second = []
    for s in range(kv_size):
        dst = lax.rem(k + s, kv_size)
        second.append(
            pltpu.make_async_remote_copy(
                src_ref=attended, dst_ref=rows_in.at[slot], send_sem=send2.at[s],
                recv_sem=recv2.at[slot], device_id={"kv": dst, "tp": owner},
            )
        )
    for c in second[1:]:
        c.start()

    @pl.when(owner != j)
    def _():
        second[0].start()

    @pl.when(owner == j)
    def _():
        rows_in[slot] = result

    final = inbox[0][0:1, width:]
    for i in range(1, kv_size):
        final = jnp.minimum(final, inbox[i][0:1, width:])
    for b in range(seqs):
        at = (2 + b) * heads
        column = jnp.concatenate([final[:, at + h : at + h + 1] for h in range(heads)], axis=0)
        new_gates[b] = jnp.where(mask[b] > 0.5, base[b] + column, base[b])

    for s in range(1, tp_size):
        src = lax.rem(j + tp_size - s, tp_size)
        pltpu.make_async_remote_copy(
            src_ref=weight, dst_ref=weights_in.at[src], send_sem=send3.at[s],
            recv_sem=recv3.at[src], device_id={"tp": src},
        ).wait_recv()
    for i in range(slots):
        from_k = j * per_owner + i % per_owner
        from_j = i // per_owner

        @pl.when(jnp.logical_or(from_k != k, from_j != j))
        def _():
            pltpu.make_async_remote_copy(
                src_ref=attended, dst_ref=rows_in.at[i], send_sem=send2.at[0],
                recv_sem=recv2.at[i], device_id={"kv": from_k, "tp": from_j},
            ).wait_recv()

    out = None
    for g in range(tp_size):
        left = jnp.concatenate(
            [rows_in[g * per_owner + i] for i in range(per_owner)], axis=0
        ).astype(BF16)
        term = jnp.dot(left, weights_in[g], preferred_element_type=F32).astype(BF16).astype(F32)
        out = term if out is None else out + term
    mixed[...] = out.astype(BF16)
    for c in first + third + second[1:]:
        c.wait_send()

    @pl.when(owner != j)
    def _():
        second[0].wait_send()


def body(
    kv_size, tp_size,
    tokens, mix_gain, query_weight, key_weight, value_weight, gate_weight, gate_bias,
    query_gain, key_gain, cache_keys, cache_values, cached_gates, filled, accepted,
    parents, out_weight,
):
    row_count, model = tokens.shape
    seqs, length, width = cache_keys.shape
    heads = cached_gates.shape[1]
    props = parents.shape[1]
    vm = pl.BlockSpec(memory_space=VMEM)
    sm = pl.BlockSpec(memory_space=pltpu.SMEM)
    hbm = pl.BlockSpec(memory_space=pl.ANY)
    wide = width + LANES
    message, tree, base, mask, new_keys, new_values = pl.pallas_call(
        head_kernel,
        out_shape=(
            jax.ShapeDtypeStruct((row_count, wide), F32),
            jax.ShapeDtypeStruct((row_count, wide), F32),
            jax.ShapeDtypeStruct(cached_gates.shape, F32),
            jax.ShapeDtypeStruct(cached_gates.shape, F32),
            jax.ShapeDtypeStruct(cache_keys.shape, BF16),
            jax.ShapeDtypeStruct(cache_values.shape, BF16),
        ),
        in_specs=[vm] * 8 + [sm] * 2 + [hbm] * 5,
        out_specs=[vm] * 4 + [hbm] * 2,
        scratch_shapes=[
            VMEM((3, model, width), BF16),
            VMEM(cache_keys.shape, BF16),
            VMEM(cache_values.shape, BF16),
            pltpu.SemaphoreType.DMA((3,)),
            pltpu.SemaphoreType.DMA((seqs,)),
            pltpu.SemaphoreType.DMA((seqs,)),
            pltpu.SemaphoreType.DMA((2, seqs)),
        ],
        compiler_params=pltpu.CompilerParams(vmem_limit_bytes=24 * 2**20),
        cost_estimate=pl.CostEstimate(
            flops=500_000_000, bytes_accessed=8 * 2**20, transcendentals=0
        ),
        name="head",
    )(
        tokens, mix_gain.reshape(1, -1), gate_weight, gate_bias.reshape(1, -1),
        query_gain.reshape(1, -1), key_gain.reshape(1, -1), cached_gates, parents,
        filled, accepted, query_weight, key_weight, value_weight, cache_keys, cache_values,
    )
    piece = row_count // kv_size
    slots = tp_size * (row_count // tp_size // piece)
    dma = pltpu.SemaphoreType.DMA
    mixed, new_gates = pl.pallas_call(
        partial(tail_kernel, kv_size, tp_size, heads),
        out_shape=(
            jax.ShapeDtypeStruct((row_count // tp_size, out_weight.shape[1]), BF16),
            jax.ShapeDtypeStruct(cached_gates.shape, F32),
        ),
        in_specs=[vm] * 5,
        out_specs=[vm] * 2,
        scratch_shapes=[
            VMEM((kv_size, piece, wide), F32),
            VMEM((piece, width), F32),
            VMEM((slots, piece, width), F32),
            VMEM((tp_size,) + out_weight.shape, BF16),
            dma((kv_size,)), dma((kv_size,)), dma((kv_size,)), dma((slots,)),
            dma((tp_size,)), dma((tp_size,)),
        ],
        compiler_params=pltpu.CompilerParams(
            collective_id=0, has_side_effects=True, vmem_limit_bytes=16 * 2**20
        ),
        name="tail",
    )(
        message.reshape(kv_size, piece, wide), tree.reshape(kv_size, piece, wide), base, mask,
        out_weight,
    )
    return (mixed, new_keys, new_values, new_gates)


def solution(mesh):
    return jax.shard_map(
        partial(body, mesh.shape["kv"], mesh.shape["tp"]),
        mesh=mesh,
        in_specs=(
            P(), P(), P(None, "tp"), P(None, "tp"), P(None, "tp"), P(), P(), P(), P(),
            P(None, "kv", "tp"), P(None, "kv", "tp"), P(None, "tp", "kv"), P(), P(), P(),
            P("tp", "kv"),
        ),
        out_specs=(P("tp", "kv"), P(None, "kv", "tp"), P(None, "kv", "tp"), P(None, "tp", "kv")),
        check_vma=False,
    )
```

time: 241 us -> 32.8 us (0.14)
  other arithmetic: 86.1 us -> 0 us
  local copies, waits for them, and re-layouts: 68.4 us -> 8.6 us
  blocking collectives: 40.3 us -> 0 us
  Pallas kernels: 0 us -> 23.1 us
  waiting for transfers between devices: 17.7 us -> 0 us
  between operations: 14.5 us -> 0.82 us
  matrix products: 11.1 us -> 0 us
    scatter x34 -> x0, other arithmetic: 73.7 us -> none
    psum x2 -> x0, blocking collectives: 40.3 us -> none  [the longest x1 23.2 us: body(): lax.psum(jnp.sum(cached_gates * at_last[:, None, :], axis=2), 'kv')]
    scatter x48 -> x0, local copies, waits for them, and re-layouts: 33.6 us -> none
    pallas_call x0 -> x2, Pallas kernels: none -> 23.1 us  [the longest x1 15.5 us: body(): pl.pallas_call(partial(tail_kernel, kv_size, tp_size, heads), out_shape=(...]
    reduce_scatter x1 -> x0, waiting for transfers between devices: 17.7 us -> none  [body(): lax.psum_scatter(jnp.dot(attended, out_weight, preferred_element_type=jnp...]
    gather x45 -> x0, local copies, waits for them, and re-layouts: 15.7 us -> none  [climb_once(): lifted = jnp.take_along_axis(parents, jnp.maximum(nodes, 0), axis=1)]
    dot_general x11 -> x0, matrix products: 11.1 us -> none  [the longest x4 4.99 us: attend_one(): jnp.einsum('thd,phd->htp', query, keys_all, preferred_element_type=jnp.fl...]
    dynamic_update_slice x8 -> x0, local copies, waits for them, and re-layouts: 7.68 us -> none  [body(): lax.map(attend_one, (query_heads, joined_keys, joined_values, joined_gate...]
  transfers between devices with their start and end apart: 2 -> 0, of which waited for: 1 -> 0; matrix products, arithmetic and copies ran while one was open for 47% -> 0% of each run, Pallas kernels for 0% -> 0%
where the time goes in v1:
time: 32.8 us; the launch traced here: 32.5 us
  Pallas kernels  23.1 us (70%)
  local copies, waits for them, and re-layouts  8.6 us (26%)
  between operations  0.82 us (2%)
    pallas_call x1, Pallas kernels, body(): pl.pallas_call(partial(tail_kernel, kv_size, tp_size, heads), out_shape=(...  15.5 us
    unnamed x33, local copies, waits for them, and re-layouts  8.6 us
    pallas_call x1, Pallas kernels, body(): pl.pallas_call(head_kernel, out_shape=(jax.ShapeDtypeStruct((row_count, w...  7.55 us

profile of v1, /device:TPU:0, one launch (start us, length us, event | category | flops | bytes accessed | tf_op | source)
XLA Modules:
  0.0 32.5 jit_solution(2229720058849766569)
XLA Ops:
  0.6 0.0 copy-start.5
  0.6 0.0 copy-start.7
  0.7 0.0 copy-start.8
  0.7 0.0 copy-start.9
  0.7 0.0 copy-start.10
  0.7 0.0 copy-start.11
  0.7 0.0 copy-start.12
  0.7 0.0 copy-start.13
  0.7 0.0 copy-start.14
  0.7 1.2 %copy.20.gate_weight = bf16[2048,16]{1,0:T(8,128)(2,1)S(1)} copy(bf16[2048,16]{0,1:T(8,128)(2,1)} %param.21) | data formatting | bytes 131072 | tf_op args[5]
  2.0 0.0 copy-done.5
  2.0 0.0 copy-done.7
  2.0 0.0 copy-done.8
  2.0 0.0 copy-done.9
  2.0 0.0 copy-done.10
  2.0 0.0 copy-done.11
  2.0 0.0 copy-done.12
  2.0 0.0 copy-done.13
  2.0 0.0 copy-done.14
  2.0 0.0 copy-start
  2.1 1.2 %copy-done = bf16[2048,256]{1,0:T(8,128)(2,1)S(1)} copy-done((bf16[2048,256]{1,0:T(8,128)(2,1)S(1)}, bf16[2048,256]{1,0:T(8,128)(2,1)}, u32[]{:S(2)}) %copy-start) | copy-done | bytes 1048600
  3.3 0.0 copy-start.1
  3.3 1.2 %copy-done.1 = bf16[2048,256]{1,0:T(8,128)(2,1)S(1)} copy-done((bf16[2048,256]{1,0:T(8,128)(2,1)S(1)}, bf16[2048,256]{1,0:T(8,128)(2,1)}, u32[]{:S(2)}) %copy-start.1) | copy-done | bytes 1048600
  4.5 0.0 copy-start.2
  4.5 1.2 %copy-done.2 = bf16[2048,256]{1,0:T(8,128)(2,1)S(1)} copy-done((bf16[2048,256]{1,0:T(8,128)(2,1)S(1)}, bf16[2048,256]{1,0:T(8,128)(2,1)}, u32[]{:S(2)}) %copy-start.2) | copy-done | bytes 1048600
  5.7 0.0 copy-start.3
  5.7 1.2 %copy-done.3 = bf16[4,512,256]{2,1,0:T(8,128)(2,1)S(1)} copy-done((bf16[4,512,256]{2,1,0:T(8,128)(2,1)S(1)}, bf16[4,512,256]{2,1,0:T(8,128)(2,1)}, u32[]{:S(2)}) %copy-start.3) | copy-done | bytes 1048600
  7.0 0.0 copy-start.4
  7.0 1.2 %copy-done.4 = bf16[4,512,256]{2,1,0:T(8,128)(2,1)S(1)} copy-done((bf16[4,512,256]{2,1,0:T(8,128)(2,1)S(1)}, bf16[4,512,256]{2,1,0:T(8,128)(2,1)}, u32[]{:S(2)}) %copy-start.4) | copy-done | bytes 1048600
  8.2 0.0 copy-start.6
  8.2 7.5 %head.1 = (f32[64,384]{1,0:T(8,128)S(1)}, f32[64,384]{1,0:T(8,128)S(1)}, f32[4,4,512]{2,1,0:T(4,128)S(1)}, f32[4,4,512]{2,1,0:T(4,128)S(1)}, bf16[4,512,256]{2,1,0:T(8,128)(2,1)}, /*index=5*/bf16[4,512,256]{2,1,0:T(8,128)(2,1)}) custom-call(bf16[64,2048]{1,0:T(8,128)(2,1)S(1)} %copy-done.5, f32[1,2048]{1,0:T(1,128)S(1)} %bitcast.8, ...), custom_call_target="tpu_custom_call" | custom-call | flops 500000000 | bytes 8388608 | tf_op jit(solution)/shard_map/head/pallas_call | solution.py:354
  15.7 0.0 copy-done.6
  15.7 15.5 %tail.1 = (bf16[16,256]{1,0:T(8,128)(2,1)S(1)}, f32[4,4,512]{2,1,0:T(4,128)S(1)}) custom-call(f32[8,8,384]{2,1,0:T(8,128)S(1)} %bitcast.6, f32[8,8,384]{2,1,0:T(8,128)S(1)} %bitcast.7, f32[4,4,512]{2,1,0:T(4,128)S(1)} %get-tuple-element.14.base, f32[4,4,512]{2,1,0:T(4,128)S(1)} %get-tuple-element.15.mask, bf16[256,256]{1,0:T(8,128)(2,1)S(1)} %copy-done.6), custom_call_target="tpu_custom_call" | custom-call | tf_op jit(solution)/shard_map/tail/pallas_call | solution.py:388
  31.3 0.6 %copy.23 = bf16[16,256]{1,0:T(8,128)(2,1)} copy(bf16[16,256]{1,0:T(8,128)(2,1)S(1)} %get-tuple-element.24) | data formatting | bytes 16384
  31.9 0.6 %copy.24 = f32[4,4,512]{2,1,0:T(4,128)} copy(f32[4,4,512]{2,1,0:T(4,128)S(1)} %get-tuple-element.27) | data formatting | bytes 65536
Async XLA Ops:
  0.6 1.3 %copy-start.5 = (bf16[64,2048]{1,0:T(8,128)(2,1)S(1)}, bf16[64,2048]{1,0:T(8,128)(2,1)}, u32[]{:S(2)}) copy-start(bf16[64,2048]{1,0:T(8,128)(2,1)} %tokens.1) | copy-start | bytes 786436
  0.6 1.3 %copy-start.7 = (f32[4,4,512]{2,1,0:T(4,128)S(1)}, f32[4,4,512]{2,1,0:T(4,128)}, u32[]{:S(2)}) copy-start(f32[4,4,512]{2,1,0:T(4,128)} %gates.1) | copy-start | bytes 98308
  0.7 1.3 %copy-start.8 = (f32[2048]{0:T(1024)S(1)}, f32[2048]{0:T(1024)}, u32[]{:S(2)}) copy-start(f32[2048]{0:T(1024)} %param.17) | copy-start | bytes 24580
  0.7 1.3 %copy-start.9 = (s32[4,16]{1,0:T(4,128)S(1)}, s32[4,16]{1,0:T(4,128)}, u32[]{:S(2)}) copy-start(s32[4,16]{1,0:T(4,128)} %parents.1) | copy-start | bytes 772
  0.7 1.3 %copy-start.10 = (f32[16]{0:T(128)S(1)}, f32[16]{0:T(128)}, u32[]{:S(2)}) copy-start(f32[16]{0:T(128)} %param.22) | copy-start | bytes 196
  0.7 1.3 %copy-start.11 = (f32[64]{0:T(128)S(1)}, f32[64]{0:T(128)}, u32[]{:S(2)}) copy-start(f32[64]{0:T(128)} %param.23) | copy-start | bytes 772
  0.7 1.3 %copy-start.12 = (f32[64]{0:T(128)S(1)}, f32[64]{0:T(128)}, u32[]{:S(2)}) copy-start(f32[64]{0:T(128)} %param.24) | copy-start | bytes 772
  0.7 1.3 %copy-start.13 = (s32[4]{0:T(128)S(1)}, s32[4]{0:T(128)}, u32[]{:S(2)}) copy-start(s32[4]{0:T(128)} %filled.1) | copy-start | bytes 52
  0.7 1.3 %copy-start.14 = (s32[4]{0:T(128)S(1)}, s32[4]{0:T(128)}, u32[]{:S(2)}) copy-start(s32[4]{0:T(128)} %accepted.1) | copy-start | bytes 52
  2.0 1.2 %copy-start = (bf16[2048,256]{1,0:T(8,128)(2,1)S(1)}, bf16[2048,256]{1,0:T(8,128)(2,1)}, u32[]{:S(2)}) copy-start(bf16[2048,256]{1,0:T(8,128)(2,1)} %wq.1) | copy-start | bytes 3145732
  3.3 1.2 %copy-start.1 = (bf16[2048,256]{1,0:T(8,128)(2,1)S(1)}, bf16[2048,256]{1,0:T(8,128)(2,1)}, u32[]{:S(2)}) copy-start(bf16[2048,256]{1,0:T(8,128)(2,1)} %wk.1) | copy-start | bytes 3145732
  4.5 1.2 %copy-start.2 = (bf16[2048,256]{1,0:T(8,128)(2,1)S(1)}, bf16[2048,256]{1,0:T(8,128)(2,1)}, u32[]{:S(2)}) copy-start(bf16[2048,256]{1,0:T(8,128)(2,1)} %wv.1) | copy-start | bytes 3145732
  5.7 1.2 %copy-start.3 = (bf16[4,512,256]{2,1,0:T(8,128)(2,1)S(1)}, bf16[4,512,256]{2,1,0:T(8,128)(2,1)}, u32[]{:S(2)}) copy-start(bf16[4,512,256]{2,1,0:T(8,128)(2,1)} %cache_keys.1) | copy-start | bytes 3145732
  7.0 1.2 %copy-start.4 = (bf16[4,512,256]{2,1,0:T(8,128)(2,1)S(1)}, bf16[4,512,256]{2,1,0:T(8,128)(2,1)}, u32[]{:S(2)}) copy-start(bf16[4,512,256]{2,1,0:T(8,128)(2,1)} %cache_values.1) | copy-start | bytes 3145732
  8.2 7.6 %copy-start.6 = (bf16[256,256]{1,0:T(8,128)(2,1)S(1)}, bf16[256,256]{1,0:T(8,128)(2,1)}, u32[]{:S(2)}) copy-start(bf16[256,256]{1,0:T(8,128)(2,1)} %weight.1) | copy-start | bytes 393220

commit v2 on v1

--- a/solution.py
+++ b/solution.py
@@ -11,6 +11,7 @@
 SHIFT = 16.0
 FAR = float(2.0**100)
 LANES = 128
+PART = 32
 F32 = jnp.float32
 BF16 = jnp.bfloat16
 HIGH = lax.Precision.HIGHEST
@@ -24,7 +25,8 @@
 def head_kernel(
     tokens, mix_gain, gate_weight, gate_bias, query_gain, key_gain, gates, parents,
     filled, accepted, wq, wk, wv, cache_keys, cache_values,
-    message, tree, base, mask, new_keys, new_values,
+    message, queries_out, keys_out, values_out, climb_out, across_out, ancestors_out,
+    new_keys, new_values,
     wbuf, kbuf, vbuf, wsem, ksem, vsem, osem,
 ):
     kv_rank = lax.axis_index("kv")
@@ -34,6 +36,7 @@
     size = width // heads
     props = parents.shape[1]
     rows = seqs * props
+    piece = message.shape[1]
     loads = []
     for i, w in enumerate((wq, wk)):
         loads.append(pltpu.make_async_copy(w, wbuf.at[i], wsem.at[i]))
@@ -66,7 +69,12 @@
         reach *= 2
     ancestors = jnp.transpose(anc)
 
-    gate_pre = jnp.dot(scaled, gate_weight[...], preferred_element_type=F32) * row_scale
+    gate_pre = (
+        lax.dot_general(
+            scaled, gate_weight[...], (((1,), (1,)), ((), ())), preferred_element_type=F32
+        )
+        * row_scale
+    )
     gate_pre = gate_pre + gate_bias[...]
     log_gates = jnp.minimum(gate_pre, 0.0) - jnp.log1p(jnp.exp(-jnp.abs(gate_pre)))
     all_heads = log_gates.shape[1]
@@ -104,7 +112,7 @@
     block_row = iota((heads * props, width), 0) // props
     diagonal = block_head == block_row
     positions = kv_rank * length + iota((heads, length), 1)
-    lane = iota((props, LANES), 1)
+    lane = iota((props, LANES), 1) % PART
     out_copies = []
     refs = []
     for b in range(seqs):
@@ -143,8 +151,14 @@
                 side = jnp.where(
                     lane == (2 + other) * heads + h, refs[other][h : h + 1, :], side
                 )
-        message[lo : lo + props, :width] = num
-        message[lo : lo + props, width:] = side
+        high = side.astype(BF16).astype(F32)
+        middle = (side - high).astype(BF16).astype(F32)
+        low = side - high - middle
+        part = iota((props, LANES), 1) // PART
+        side = jnp.where(part == 0, high, jnp.where(part == 1, middle, low))
+        packed = jnp.concatenate([num, side], axis=1)
+        for r in range(0, props, piece):
+            message[(lo + r) // piece] = packed[r : r + piece].astype(BF16)
 
         offset = count - kv_rank * length
         start = jnp.clip((offset // props) * props, 0, length - window)
@@ -164,44 +178,21 @@
             c.start()
             out_copies.append(c)
 
-        gate_rel = positions - count
-        chosen = jnp.logical_and(gate_rel >= 0, gate_rel < props)
-        placed_gates = own
-        for t in range(props):
-            column = jnp.concatenate(
-                [climb[lo + t : lo + t + 1, h : h + 1] for h in range(heads)], axis=0
-            )
-            placed_gates = jnp.where(gate_rel == t, column, placed_gates)
-        base[b] = placed_gates
-        mask[b] = chosen.astype(F32)
-
-    tree_side = jnp.zeros((rows, LANES), F32)
-    row_lane = iota((rows, LANES), 1)
-    tree_parts = []
-    for h in range(heads):
-        scores = lax.dot_general(
-            query[h], fresh_key_heads[h], (((1,), (1,)), ((), ())), preferred_element_type=F32
-        )
-        scores = scores + climb[:, h : h + 1] - climb_across[h : h + 1, :] - SHIFT
-        weights = jnp.exp(jnp.where(ancestors > 0.5, scores, -FAR))
-        tree_side = jnp.where(row_lane == h, jnp.sum(weights, axis=1, keepdims=True), tree_side)
-        tree_parts.append(
-            jnp.dot(
-                weights.astype(BF16),
-                fresh_values[:, h * size : (h + 1) * size],
-                preferred_element_type=F32,
-            )
-        )
-    tree[:, :width] = jnp.concatenate(tree_parts, axis=1)
-    tree[:, width:] = tree_side
+    queries_out[...] = query_all
+    keys_out[...] = fresh_keys
+    values_out[...] = fresh_values
+    climb_out[...] = climb
+    across_out[...] = climb_across
+    ancestors_out[...] = ancestors
     for c in out_copies:
         c.wait()
 
 
 def tail_kernel(
-    kv_size, tp_size, heads, message, tree, base, mask, weight,
+    kv_size, tp_size, heads, message, queries, fresh_keys, fresh_values, climb, across,
+    ancestors, gates, weight, filled, accepted,
     mixed, new_gates,
-    inbox, attended, rows_in, weights_in, send1, recv1, send2, recv2, send3, recv3,
+    tree, inbox, attended, rows_in, weights_in, send1, recv1, send2, recv2, send3, recv3,
 ):
     k = lax.axis_index("kv")
     j = lax.axis_index("tp")
@@ -210,7 +201,9 @@
     piece = message.shape[1]
     width = attended.shape[1]
     size = width // heads
-    seqs = base.shape[0]
+    seqs, _, length = gates.shape
+    rows = queries.shape[0]
+    props = rows // seqs
     slots = rows_in.shape[0]
     per_owner = slots // tp_size
     owner = k // per_owner
@@ -246,6 +239,36 @@
         third.append(c)
     inbox[k] = message[k]
     weights_in[j] = weight[...]
+    side = jnp.zeros((rows, LANES), F32)
+    row_lane = iota((rows, LANES), 1)
+    tree_parts = []
+    for h in range(heads):
+        at = slice(h * size, (h + 1) * size)
+        scores = lax.dot_general(
+            queries[:, at], fresh_keys[:, at], (((1,), (1,)), ((), ())),
+            preferred_element_type=F32,
+        )
+        scores = scores + climb[:, h : h + 1] - across[h : h + 1, :] - SHIFT
+        weights = jnp.exp(jnp.where(ancestors[...] > 0.5, scores, -FAR))
+        side = jnp.where(row_lane == h, jnp.sum(weights, axis=1, keepdims=True), side)
+        tree_parts.append(
+            jnp.dot(weights.astype(BF16), fresh_values[:, at], preferred_element_type=F32)
+        )
+    packed = jnp.concatenate(tree_parts + [side], axis=1)
+    for i in range(kv_size):
+        tree[i] = packed[i * piece : (i + 1) * piece]
+    positions = k * length + iota((heads, length), 1)
+    chosen = []
+    placed = []
+    for b in range(seqs):
+        rel = positions - (filled[b] + accepted[b])
+        chosen.append(jnp.logical_and(rel >= 0, rel < props))
+        climbs = jnp.zeros((heads, length), F32)
+        for t in range(props):
+            u = b * props + t
+            column = jnp.broadcast_to(across[:heads, u : u + 1], (heads, length))
+            climbs = jnp.where(rel == t, column, climbs)
+        placed.append(climbs)
     for s in range(1, kv_size):
         src = lax.rem(k + kv_size - s, kv_size)
         pltpu.make_async_remote_copy(
@@ -253,15 +276,25 @@
             recv_sem=recv1.at[src], device_id={"kv": src},
         ).wait_recv()
 
-    last = inbox[0][:, width + heads : width + 2 * heads]
-    for i in range(1, kv_size):
-        last = jnp.minimum(last, inbox[i][:, width + heads : width + 2 * heads])
-    scales = []
+    parts = []
+    sides = []
+    for i in range(kv_size):
+        got = inbox[i].astype(F32)
+        parts.append(got[:, :width])
+        side = got[:, width:]
+        sides.append(
+            side[:, :PART] + side[:, PART : 2 * PART] + side[:, 2 * PART : 3 * PART]
+        )
+    final = sides[0]
+    for side in sides[1:]:
+        final = jnp.minimum(final, side)
+    last = final[:, heads : 2 * heads]
     own_tree = tree[k]
     den = own_tree[:, width : width + heads]
-    for i in range(kv_size):
-        scale = jnp.exp(last - inbox[i][:, width + heads : width + 2 * heads])
-        den = den + scale * inbox[i][:, width : width + heads]
+    scales = []
+    for side in sides:
+        scale = jnp.exp(last - side[:, heads : 2 * heads])
+        den = den + scale * side[:, :heads]
         scales.append(scale)
 
     def spread(x):
@@ -271,8 +304,8 @@
 
     num = own_tree[:, :width]
     for i in range(kv_size):
-        num = num + spread(scales[i]) * inbox[i][:, :width]
-    result = (num / spread(den)).astype(BF16).astype(F32)
+        num = num + spread(scales[i]) * parts[i]
+    result = (num / spread(den)).astype(BF16)
     attended[...] = result
 
     slot = j * per_owner + lax.rem(k, per_owner)
@@ -296,13 +329,11 @@
     def _():
         rows_in[slot] = result
 
-    final = inbox[0][0:1, width:]
-    for i in range(1, kv_size):
-        final = jnp.minimum(final, inbox[i][0:1, width:])
+    final = final[0:1, :]
     for b in range(seqs):
         at = (2 + b) * heads
         column = jnp.concatenate([final[:, at + h : at + h + 1] for h in range(heads)], axis=0)
-        new_gates[b] = jnp.where(mask[b] > 0.5, base[b] + column, base[b])
+        new_gates[b] = jnp.where(chosen[b], placed[b] + column, gates[b])
 
     for s in range(1, tp_size):
         src = lax.rem(j + tp_size - s, tp_size)
@@ -324,7 +355,7 @@
     out = None
     for g in range(tp_size):
         left = jnp.concatenate(
-            [rows_in[g * per_owner + i] for i in range(per_owner)], axis=0
+            [rows_in[g * per_owner + i].astype(F32) for i in range(per_owner)], axis=0
         ).astype(BF16)
         term = jnp.dot(left, weights_in[g], preferred_element_type=F32).astype(BF16).astype(F32)
         out = term if out is None else out + term
@@ -351,18 +382,22 @@
     sm = pl.BlockSpec(memory_space=pltpu.SMEM)
     hbm = pl.BlockSpec(memory_space=pl.ANY)
     wide = width + LANES
-    message, tree, base, mask, new_keys, new_values = pl.pallas_call(
+    piece = row_count // kv_size
+    message, *carried, new_keys, new_values = pl.pallas_call(
         head_kernel,
         out_shape=(
-            jax.ShapeDtypeStruct((row_count, wide), F32),
-            jax.ShapeDtypeStruct((row_count, wide), F32),
-            jax.ShapeDtypeStruct(cached_gates.shape, F32),
-            jax.ShapeDtypeStruct(cached_gates.shape, F32),
+            jax.ShapeDtypeStruct((kv_size, piece, wide), BF16),
+            jax.ShapeDtypeStruct((row_count, width), BF16),
+            jax.ShapeDtypeStruct((row_count, width), BF16),
+            jax.ShapeDtypeStruct((row_count, width), BF16),
+            jax.ShapeDtypeStruct((row_count, LANES), F32),
+            jax.ShapeDtypeStruct((LANES, row_count), F32),
+            jax.ShapeDtypeStruct((row_count, row_count), F32),
             jax.ShapeDtypeStruct(cache_keys.shape, BF16),
             jax.ShapeDtypeStruct(cache_values.shape, BF16),
         ),
         in_specs=[vm] * 8 + [sm] * 2 + [hbm] * 5,
-        out_specs=[vm] * 4 + [hbm] * 2,
+        out_specs=[vm] * 7 + [hbm] * 2,
         scratch_shapes=[
             VMEM((3, model, width), BF16),
             VMEM(cache_keys.shape, BF16),
@@ -372,17 +407,16 @@
             pltpu.SemaphoreType.DMA((seqs,)),
             pltpu.SemaphoreType.DMA((2, seqs)),
         ],
-        compiler_params=pltpu.CompilerParams(vmem_limit_bytes=24 * 2**20),
+        compiler_params=pltpu.CompilerParams(vmem_limit_bytes=int(53.5 * 2**20)),
         cost_estimate=pl.CostEstimate(
             flops=500_000_000, bytes_accessed=8 * 2**20, transcendentals=0
         ),
         name="head",
     )(
-        tokens, mix_gain.reshape(1, -1), gate_weight, gate_bias.reshape(1, -1),
+        tokens, mix_gain.reshape(1, -1), jnp.transpose(gate_weight), gate_bias.reshape(1, -1),
         query_gain.reshape(1, -1), key_gain.reshape(1, -1), cached_gates, parents,
         filled, accepted, query_weight, key_weight, value_weight, cache_keys, cache_values,
     )
-    piece = row_count // kv_size
     slots = tp_size * (row_count // tp_size // piece)
     dma = pltpu.SemaphoreType.DMA
     mixed, new_gates = pl.pallas_call(
@@ -391,12 +425,13 @@
             jax.ShapeDtypeStruct((row_count // tp_size, out_weight.shape[1]), BF16),
             jax.ShapeDtypeStruct(cached_gates.shape, F32),
         ),
-        in_specs=[vm] * 5,
+        in_specs=[vm] * 9 + [sm] * 2,
         out_specs=[vm] * 2,
         scratch_shapes=[
             VMEM((kv_size, piece, wide), F32),
-            VMEM((piece, width), F32),
-            VMEM((slots, piece, width), F32),
+            VMEM((kv_size, piece, wide), BF16),
+            VMEM((piece, width), BF16),
+            VMEM((slots, piece, width), BF16),
             VMEM((tp_size,) + out_weight.shape, BF16),
             dma((kv_size,)), dma((kv_size,)), dma((kv_size,)), dma((slots,)),
             dma((tp_size,)), dma((tp_size,)),
@@ -406,8 +441,7 @@
         ),
         name="tail",
     )(
-        message.reshape(kv_size, piece, wide), tree.reshape(kv_size, piece, wide), base, mask,
-        out_weight,
+        message, *carried, cached_gates, out_weight, filled, accepted,
     )
     return (mixed, new_keys, new_values, new_gates)
 

time: 32.8 us -> 30.4 us (0.927)
  local copies, waits for them, and re-layouts: 8.6 us -> 6.14 us
    unnamed x33 -> x22, local copies, waits for them, and re-layouts: 8.6 us -> 6.14 us
where the time goes in v2:
time: 30.4 us; the launch traced here: 30.1 us
  Pallas kernels  23.3 us (77%)
  local copies, waits for them, and re-layouts  6.14 us (20%)
  between operations  0.69 us (2%)
    pallas_call x1, Pallas kernels, body(): pl.pallas_call(partial(tail_kernel, kv_size, tp_size, heads), out_shape=(...  15.8 us
    pallas_call x1, Pallas kernels, body(): pl.pallas_call(head_kernel, out_shape=(jax.ShapeDtypeStruct((kv_size, pie...  7.52 us
    unnamed x22, local copies, waits for them, and re-layouts  6.14 us

profile of v2, /device:TPU:0, one launch (start us, length us, event | category | flops | bytes accessed | tf_op | source)
XLA Modules:
  0.0 30.1 jit_solution(763571633558974664)
XLA Ops:
  0.6 0.0 copy-start.3
  0.6 0.0 copy-start.5
  0.7 0.0 copy-start.6
  0.7 0.7 %copy-done.3 = f32[2048]{0:T(1024)S(1)} copy-done((f32[2048]{0:T(1024)S(1)}, f32[2048]{0:T(1024)}, u32[]{:S(2)}) %copy-start.3) | copy-done | bytes 8216
  1.3 0.0 copy-done.5
  1.3 0.0 copy-done.6
  1.3 0.0 copy-start
  1.3 0.8 %copy-done = f32[4,4,512]{2,1,0:T(4,128)S(1)} copy-done((f32[4,4,512]{2,1,0:T(4,128)S(1)}, f32[4,4,512]{2,1,0:T(4,128)}, u32[]{:S(2)}) %copy-start) | copy-done | bytes 32792
  2.1 0.0 copy-start.2
  2.1 0.8 %copy-done.2 = bf16[2048,16]{0,1:T(8,128)(2,1)S(1)} copy-done((bf16[2048,16]{0,1:T(8,128)(2,1)S(1)}, bf16[2048,16]{0,1:T(8,128)(2,1)}, u32[]{:S(2)}) %copy-start.2) | copy-done | bytes 65560
  2.9 0.0 copy-start.4
  2.9 0.7 %copy-done.4 = s32[4,16]{1,0:T(4,128)S(1)} copy-done((s32[4,16]{1,0:T(4,128)S(1)}, s32[4,16]{1,0:T(4,128)}, u32[]{:S(2)}) %copy-start.4) | copy-done | bytes 280
  3.6 0.0 copy-start.7
  3.6 0.7 %copy-done.7 = f32[16]{0:T(128)S(1)} copy-done((f32[16]{0:T(128)S(1)}, f32[16]{0:T(128)}, u32[]{:S(2)}) %copy-start.7) | copy-done | bytes 88
  4.3 0.0 copy-start.8
  4.3 0.7 %copy-done.8 = f32[64]{0:T(128)S(1)} copy-done((f32[64]{0:T(128)S(1)}, f32[64]{0:T(128)}, u32[]{:S(2)}) %copy-start.8) | copy-done | bytes 280
  4.9 0.0 copy-start.9
  4.9 0.7 %copy-done.9 = f32[64]{0:T(128)S(1)} copy-done((f32[64]{0:T(128)S(1)}, f32[64]{0:T(128)}, u32[]{:S(2)}) %copy-start.9) | copy-done | bytes 280
  5.6 0.0 copy-start.1
  5.6 7.5 %head.1 = (bf16[8,8,384]{2,1,0:T(8,128)(2,1)S(1)}, bf16[64,256]{1,0:T(8,128)(2,1)S(1)}, bf16[64,256]{1,0:T(8,128)(2,1)S(1)}, bf16[64,256]{1,0:T(8,128)(2,1)S(1)}...) custom-call(bf16[64,2048]{1,0:T(8,128)(2,1)} %tokens.1, ...), custom_call_target="tpu_custom_call" | custom-call | flops 500000000 | bytes 8388608 | tf_op jit(solution)/shard_map/head/pallas_call | solution.py:386
  13.1 0.0 copy-done.1
  13.1 15.8 %tail.1 = (bf16[16,256]{1,0:T(8,128)(2,1)S(1)}, f32[4,4,512]{2,1,0:T(4,128)S(1)}) custom-call(bf16[8,8,384]{2,1,0:T(8,128)(2,1)S(1)} %get-tuple-element.15.message, bf16[64,256]{1,0:T(8,128)(2,1)S(1)} %get-tuple-element.16.queries, bf16[64,256]{1,0:T(8,128)(2,1)S(1)} %get-tuple-element.17.fresh_keys, bf16[64,256]{1,0:T(8,128)(2,1)S(1)} %get-tuple-element.18.fresh_values, ...), custom_call_target="tpu_custom_call" | custom-call | tf_op jit(solution)/shard_map/tail/pallas_call | solution.py:422
  28.9 0.6 %copy.22 = bf16[16,256]{1,0:T(8,128)(2,1)} copy(bf16[16,256]{1,0:T(8,128)(2,1)S(1)} %get-tuple-element.30) | data formatting | bytes 16384
  29.5 0.6 %copy.23 = f32[4,4,512]{2,1,0:T(4,128)} copy(f32[4,4,512]{2,1,0:T(4,128)S(1)} %get-tuple-element.33) | data formatting | bytes 65536
Async XLA Ops:
  0.6 0.7 %copy-start.3 = (f32[2048]{0:T(1024)S(1)}, f32[2048]{0:T(1024)}, u32[]{:S(2)}) copy-start(f32[2048]{0:T(1024)} %param.17) | copy-start | bytes 24580
  0.6 0.7 %copy-start.5 = (s32[4]{0:T(128)S(1)}, s32[4]{0:T(128)}, u32[]{:S(2)}) copy-start(s32[4]{0:T(128)} %filled.3) | copy-start | bytes 52
  0.7 0.7 %copy-start.6 = (s32[4]{0:T(128)S(1)}, s32[4]{0:T(128)}, u32[]{:S(2)}) copy-start(s32[4]{0:T(128)} %accepted.3) | copy-start | bytes 52
  1.3 0.8 %copy-start = (f32[4,4,512]{2,1,0:T(4,128)S(1)}, f32[4,4,512]{2,1,0:T(4,128)}, u32[]{:S(2)}) copy-start(f32[4,4,512]{2,1,0:T(4,128)} %gates.3) | copy-start | bytes 98308
  2.1 0.8 %copy-start.2 = (bf16[2048,16]{0,1:T(8,128)(2,1)S(1)}, bf16[2048,16]{0,1:T(8,128)(2,1)}, u32[]{:S(2)}) copy-start(bf16[2048,16]{0,1:T(8,128)(2,1)} %param.21) | copy-start | bytes 196612
  2.9 0.7 %copy-start.4 = (s32[4,16]{1,0:T(4,128)S(1)}, s32[4,16]{1,0:T(4,128)}, u32[]{:S(2)}) copy-start(s32[4,16]{1,0:T(4,128)} %parents.1) | copy-start | bytes 772
  3.6 0.7 %copy-start.7 = (f32[16]{0:T(128)S(1)}, f32[16]{0:T(128)}, u32[]{:S(2)}) copy-start(f32[16]{0:T(128)} %param.22) | copy-start | bytes 196
  4.3 0.7 %copy-start.8 = (f32[64]{0:T(128)S(1)}, f32[64]{0:T(128)}, u32[]{:S(2)}) copy-start(f32[64]{0:T(128)} %param.23) | copy-start | bytes 772
  4.9 0.7 %copy-start.9 = (f32[64]{0:T(128)S(1)}, f32[64]{0:T(128)}, u32[]{:S(2)}) copy-start(f32[64]{0:T(128)} %param.24) | copy-start | bytes 772
  5.6 7.5 %copy-start.1 = (bf16[256,256]{1,0:T(8,128)(2,1)S(1)}, bf16[256,256]{1,0:T(8,128)(2,1)}, u32[]{:S(2)}) copy-start(bf16[256,256]{1,0:T(8,128)(2,1)} %weight.1) | copy-start | bytes 393220

commit v3 on v2

--- a/solution.py
+++ b/solution.py
@@ -407,7 +407,7 @@
             pltpu.SemaphoreType.DMA((seqs,)),
             pltpu.SemaphoreType.DMA((2, seqs)),
         ],
-        compiler_params=pltpu.CompilerParams(vmem_limit_bytes=int(53.5 * 2**20)),
+        compiler_params=pltpu.CompilerParams(vmem_limit_bytes=62 * 2**20),
         cost_estimate=pl.CostEstimate(
             flops=500_000_000, bytes_accessed=8 * 2**20, transcendentals=0
         ),
@@ -437,7 +437,7 @@
             dma((tp_size,)), dma((tp_size,)),
         ],
         compiler_params=pltpu.CompilerParams(
-            collective_id=0, has_side_effects=True, vmem_limit_bytes=16 * 2**20
+            collective_id=0, has_side_effects=True, vmem_limit_bytes=62 * 2**20
         ),
         name="tail",
     )(

time: 30.4 us -> 28.3 us (0.931)
  local copies, waits for them, and re-layouts: 6.14 us -> 2.67 us
  Pallas kernels: 23.3 us -> 24.7 us
    unnamed x22 -> x2, local copies, waits for them, and re-layouts: 6.14 us -> 2.67 us
    pallas_call x1, Pallas kernels: 15.8 us -> 16.9 us  [body(): pl.pallas_call(partial(tail_kernel, kv_size, tp_size, heads), out_shape=(...]
    pallas_call x1, Pallas kernels: 7.52 us -> 7.83 us  [body(): pl.pallas_call(head_kernel, out_shape=(jax.ShapeDtypeStruct((kv_size, pie...]
where the time goes in v3:
time: 28.3 us; the launch traced here: 28.1 us
  Pallas kernels  24.7 us (87%)
  local copies, waits for them, and re-layouts  2.67 us (9%)
  between operations  0.65 us (2%)
    pallas_call x1, Pallas kernels, body(): pl.pallas_call(partial(tail_kernel, kv_size, tp_size, heads), out_shape=(...  16.9 us
    pallas_call x1, Pallas kernels, body(): pl.pallas_call(head_kernel, out_shape=(jax.ShapeDtypeStruct((kv_size, pie...  7.83 us
    unnamed x2, local copies, waits for them, and re-layouts  2.67 us

profile of v3, /device:TPU:0, one launch (start us, length us, event | category | flops | bytes accessed | tf_op | source)
XLA Modules:
  0.0 28.1 jit_solution(13019178729239990333)
XLA Ops:
  0.6 7.8 %head.1 = (bf16[8,8,384]{2,1,0:T(8,128)(2,1)}, bf16[64,256]{1,0:T(8,128)(2,1)}, bf16[64,256]{1,0:T(8,128)(2,1)}, bf16[64,256]{1,0:T(8,128)(2,1)}, f32[64,128]{1,...) custom-call(bf16[64,2048]{1,0:T(8,128)(2,1)} %tokens.1, ...), custom_call_target="tpu_custom_call" | custom-call | flops 500000000 | bytes 8388608 | tf_op jit(solution)/shard_map/head/pallas_call | solution.py:386
  8.5 16.9 %tail.1 = (bf16[16,256]{1,0:T(8,128)(2,1)}, f32[4,4,512]{2,1,0:T(4,128)}) custom-call(bf16[8,8,384]{2,1,0:T(8,128)(2,1)} %get-tuple-element.15.message, bf16[64,256]{1,0:T(8,128)(2,1)} %get-tuple-element.16.queries, bf16[64,256]{1,0:T(8,128)(2,1)} %get-tuple-element.17.fresh_keys, bf16[64,256]{1,0:T(8,128)(2,1)} %get-tuple-element.18.fresh_values, ...), custom_call_target="tpu_custom_call" | custom-call | tf_op jit(solution)/shard_map/tail/pallas_call | solution.py:422
  25.4 1.3 %copy.22 = bf16[16,256]{1,0:T(8,128)(2,1)} copy(bf16[16,256]{1,0:T(8,128)(2,1)} %get-tuple-element.30) | data formatting | bytes 16384
  26.7 1.4 %copy.23 = f32[4,4,512]{2,1,0:T(4,128)} copy(f32[4,4,512]{2,1,0:T(4,128)} %get-tuple-element.33) | data formatting | bytes 65536
